TPU v7x, 256 devices: a whole 4x4x8 slice. The times are simulated.
256 devices in a mesh: fs: 32 (over z, x), tp: 8 (over y, core).
Axes of the slice: x: 4, y: 4, z: 8, core: 2. Of those that a mesh axis runs over, the one named last changes fastest.
Arguments:
- tokens: bfloat16 [6144, 2048], P('fs'), may hold values from -6 to 6
- norm_gain: float32 [2048], P('fs'), may hold values from 0.1 to 1.9
- expert_gate: float32 [64, 2048, 1024], P(None, 'fs', 'tp'), may hold values from -0.125 to 0.125
- expert_up: float32 [64, 2048, 1024], P(None, 'fs', 'tp'), may hold values from -0.125 to 0.125
- expert_down: float32 [64, 1024, 2048], P(None, 'fs', 'tp'), may hold values from -0.1875 to 0.1875
- shared_gate: float32 [2048, 1024], P('fs', 'tp'), may hold values from -0.125 to 0.125
- shared_up: float32 [2048, 1024], P('fs', 'tp'), may hold values from -0.125 to 0.125
- shared_down: float32 [1024, 2048], P('fs', 'tp'), may hold values from -0.1875 to 0.1875
- expert_ids: int32 [6144, 8], P('fs'), may hold values from 0 to 63, all different within a row; in each aligned block of 192 rows (0 to 191, 192 to 383, ...) at most 48 rows name the same one
- route_weights: float32 [6144, 8], P('fs'), may hold values from 0.25 to 1
Outputs:
- gate_ready: bfloat16 [64, 2048, 1024], P('fs', None, 'tp')
- up_ready: bfloat16 [64, 2048, 1024], P('fs', None, 'tp')
- down_ready: bfloat16 [64, 1024, 2048], P('fs', None, 'tp')
- shared_gate_ready: bfloat16 [2048, 1024], P(None, 'tp')
- shared_up_ready: bfloat16 [2048, 1024], P(None, 'tp')
- shared_down_ready: bfloat16 [1024, 2048], P(None, 'tp')
- mixed: bfloat16 [6144, 2048], P('fs', 'tp')
Inputs may be any that keep to these rules, and one draw needn't show every extreme that they name: `expert_ids`: each row names 8 different experts. Among the 192 rows of one index of fs no expert is named more than 48 times, and in every draw some expert is named exactly 48 times there.
All inputs are finite; a program needn't handle non-finite values.
Results may differ from a plain program's by a relative error of at most 0.0085.
Values may be sent and summed in bfloat16 or wider, within the bound.
A program may use at most 128 MiB of HBM per device.

v0:
```python
import jax
import jax.numpy as jnp
from jax import lax
from jax.sharding import PartitionSpec as P

TOP_K = 8
EPS = 1e-06


def cut_along(shard, dim, size):
    before, after = (shard.shape[:dim], shard.shape[dim + 1 :])
    return jnp.moveaxis(shard.reshape(*before, size, -1, *after), dim, 0)


def piece_ends(length, count):
    turn = length // count
    if turn >= 8:
        turn -= turn % 8
    return [turn * k for k in range(1, count)]


def in_order(parts, dim):
    parts = jnp.moveaxis(parts, 0, dim)
    shape = parts.shape
    return parts.reshape(*shape[:dim], shape[dim] * shape[dim + 1], *shape[dim + 2 :])


def several_exchanges(shard, axis, pieces, split_dim, concat_dim):
    parts = cut_along(shard, split_dim, lax.axis_size(axis))
    split_at = max(range(1, max(2, parts.ndim - 1)), key=lambda d: parts.shape[d])
    done = []
    for share in jnp.split(parts, piece_ends(parts.shape[split_at], pieces), axis=split_at):
        if share.size:
            done.append(lax.all_to_all(share, axis, split_axis=0, concat_axis=0, tiled=True))
    return in_order(jnp.concatenate(done, axis=split_at), concat_dim)


def side_by_side(arrays, axis, dim, along):
    ends, at = ([], 0)
    for a in arrays[:-1]:
        at += a.shape[along]
        ends.append(at)
    both = jnp.concatenate(arrays, axis=along)
    return tuple(jnp.split(lax.all_gather(both, axis, axis=dim, tiled=True), ends, axis=along))


def turned_gather(arrays, axis, dims):
    turned = [jnp.moveaxis(a, dim, 0) for a, dim in zip(arrays, dims)]
    widths = [t[0].size for t in turned]
    both = jnp.concatenate([t.reshape(-1, w) for t, w in zip(turned, widths)], axis=1)
    result = lax.all_gather(both, axis, axis=0, tiled=True)
    parts = jnp.split(result, [sum(widths[:k]) for k in range(1, len(widths))], axis=1)
    return tuple(
        (
            jnp.moveaxis(b.reshape(-1, *t.shape[1:]), 0, dim)
            for b, t, dim in zip(parts, turned, dims)
        )
    )


def expert_hidden(rows, gate_new, up_new):
    first = jnp.einsum("secn,enf->secf", rows, gate_new, preferred_element_type=jnp.float32)
    second = jnp.einsum("secn,enf->secf", rows, up_new, preferred_element_type=jnp.float32)
    return (jax.nn.silu(first) * second).astype(jnp.bfloat16)


def body(
    tokens,
    norm_gain,
    expert_gate,
    expert_up,
    expert_down,
    shared_gate,
    shared_up,
    shared_down,
    expert_ids,
    route_weights,
):
    groups = lax.axis_size("fs")
    experts = expert_gate.shape[0]
    per_group = experts // groups
    tok_count = tokens.shape[0]
    capacity = 2 * tok_count * TOP_K // experts
    gate_local = (expert_gate * norm_gain[None, :, None]).astype(jnp.bfloat16)
    up_local = (expert_up * norm_gain[None, :, None]).astype(jnp.bfloat16)
    down_local = expert_down.astype(jnp.bfloat16)
    gate_local = gate_local.reshape((groups, per_group) + gate_local.shape[1:])
    up_local = up_local.reshape((groups, per_group) + up_local.shape[1:])
    down_local = down_local.reshape((groups, per_group) + down_local.shape[1:])
    shared_first_local = (shared_gate * norm_gain[:, None]).astype(jnp.bfloat16)
    shared_second_local = (shared_up * norm_gain[:, None]).astype(jnp.bfloat16)
    shared_third_local = shared_down.astype(jnp.bfloat16)
    gate_moved, up_moved = (
        several_exchanges(gate_local, "fs", 2, 0, 2),
        several_exchanges(up_local, "fs", 2, 0, 2),
    )
    gate_ready = gate_moved[0]
    up_ready = up_moved[0]
    shared_gate_ready, shared_up_ready, shared_down_ready = (
        *side_by_side((shared_first_local, shared_second_local), "fs", 0, 1),
        lax.all_gather(shared_third_local, "fs", axis=0, tiled=True),
    )
    wide = tokens.astype(jnp.float32)
    normed = (wide * lax.rsqrt(jnp.mean(wide * wide, axis=-1, keepdims=True) + EPS)).astype(
        jnp.bfloat16
    )
    chosen = expert_ids.reshape(-1)
    onehot = (chosen[:, None] == jnp.arange(experts, dtype=jnp.int32)[None, :]).astype(jnp.int32)
    ranks = jnp.sum(jnp.cumsum(onehot, axis=0) * onehot, axis=1) - 1
    owners = jnp.arange(tok_count * TOP_K, dtype=jnp.int32) // TOP_K
    slot_token = jnp.zeros((experts, capacity), jnp.int32).at[chosen, ranks].set(owners)
    outgoing = normed[slot_token.reshape(-1)].reshape(groups, per_group, capacity, normed.shape[1])
    share = capacity // lax.axis_size("tp")
    mine = lax.dynamic_slice_in_dim(outgoing, lax.axis_index("tp") * share, share, 2)
    arrived = lax.all_to_all(mine, "fs", split_axis=0, concat_axis=0, tiled=True)
    hidden = expert_hidden(lax.all_gather(arrived, "tp", axis=2, tiled=True), gate_ready, up_ready)
    shared_first = jnp.dot(normed, shared_gate_ready, preferred_element_type=jnp.float32)
    shared_second = jnp.dot(normed, shared_up_ready, preferred_element_type=jnp.float32)
    shared_hidden = (jax.nn.silu(shared_first) * shared_second).astype(jnp.bfloat16)[None, None]
    down_moved = lax.all_to_all(down_local, "fs", split_axis=0, concat_axis=2, tiled=True)
    down_ready = down_moved[0]
    columns = down_ready.shape[2]
    routed_piece, shared_piece = turned_gather((hidden, shared_hidden), "tp", (3, 3))
    routed_total = jnp.einsum(
        "secf,efd->secd", routed_piece, down_ready, preferred_element_type=jnp.float32
    )
    shared_total = jnp.einsum(
        "abtf,fd->abtd", shared_piece, shared_down_ready, preferred_element_type=jnp.float32
    )
    returned = lax.all_to_all(
        routed_total.astype(jnp.bfloat16), "fs", split_axis=0, concat_axis=0, tiled=True
    )
    returned = returned.reshape(experts * capacity, columns)
    picked = (
        returned[chosen * capacity + ranks].astype(jnp.float32).reshape(tok_count, TOP_K, columns)
    )
    routed = jnp.sum(picked * route_weights[:, :, None], axis=1)
    mixed = (shared_total[0, 0] + routed).astype(jnp.bfloat16)
    return (
        gate_ready,
        up_ready,
        down_ready,
        shared_gate_ready,
        shared_up_ready,
        shared_down_ready,
        mixed,
    )


def solution(mesh):
    in_specs = (
        P("fs", None),
        P("fs"),
        P(None, "fs", "tp"),
        P(None, "fs", "tp"),
        P(None, "fs", "tp"),
        P("fs", "tp"),
        P("fs", "tp"),
        P("fs", "tp"),
        P("fs", None),
        P("fs", None),
    )
    out_specs = (
        P("fs", None, "tp"),
        P("fs", None, "tp"),
        P("fs", None, "tp"),
        P(None, "tp"),
        P(None, "tp"),
        P(None, "tp"),
        P("fs", "tp"),
    )
    return jax.shard_map(body, mesh=mesh, in_specs=in_specs, out_specs=out_specs, check_vma=False)
```

profile of v0, /device:TPU:32, one launch (start us, length us, event | category | flops | bytes accessed | tf_op | source)
XLA Modules:
  0.0 414.8 jit_solution(16375426263147226016)
XLA Ops:
  8.4 18.1 %reduce-window.6 = s32[64,12,128]{2,1,0:T(8,128)S(1)} reduce-window(s32[64,12,128]{2,1,0:T(8,128)S(1)} %fusion.25, s32[]{:T(128)} %constant.44.clone.1), window={size=1x1x128 pad=0_0x0_0x127_0}, to_apply=%region_1.0 | reduce-window | flops 12484608 | bytes 786436 | tf_op jit(solution)/shard_map/reduce-window
  27.8 6.2 %scatter_custom_fusion = s32[3072]{0:T(1024)S(1)} fusion(s32[1536]{0:T(1024)S(1)} %get-tuple-element.23, s32[1536]{0:T(1024)S(1)} %get-tuple-element.22, s32[]{:T(128)} %constant.44.clone.1), kind=kCustom, calls=%fused_computation.63 | custom fusion | bytes 12292
  34.7 15.9 %gather_fusion = bf16[3072,2048]{1,0:T(8,128)(2,1)} fusion(bf16[192,2048]{1,0:T(8,128)(2,1)S(1)} %fusion.11, s32[3072]{0:T(1024)S(1)} %broadcast_clamp_fusion), kind=kCustom, calls=%fused_computation | custom fusion | bytes 25178112 | tf_op jit(solution)/shard_map/gather | solution.py:112
  50.7 3.0 constant_dynamic-slice_fusion
  53.7 2.8 copy.64
  56.5 11.3 %all-to-all-start.5 = ((bf16[32,2,6,2048]{3,1,2,0:T(2,128)(2,1)}), bf16[32,2,6,2048]{3,1,2,0:T(2,128)(2,1)S(1)}, u32[]{:S(2)}, u32[]{:S(2)}) async-start(bf16[32,2,6,2048]{3,1,2,0:T(2,128)(2,1)} %copy.64), calls=%async_computation.5 | async-start | bytes 3145728 | tf_op jit(solution)/shard_map/all_to_all | solution.py:115
  68.6 38.4 %all-to-all-done.5 = bf16[32,2,6,2048]{3,1,2,0:T(2,128)(2,1)S(1)} async-done(((bf16[32,2,6,2048]{3,1,2,0:T(2,128)(2,1)}), bf16[32,2,6,2048]{3,1,2,0:T(2,128)(2,1)S(1)}, u32[]{:S(2)}, u32[]{:S(2)}) %all-to-all-start.5) | async-done | bytes 1572896 | tf_op jit(solution)/shard_map/all_to_all | solution.py:115
  107.1 2.0 copy.65
  109.1 2.8 multiply_convert_fusion
  112.0 0.9 fusion.36
  112.9 23.9 %all_to_all.45 = bf16[32,1,2,32,128]{4,3,2,1,0:T(8,128)(2,1)S(1)} all-to-all(bf16[32,1,2,32,128]{4,3,2,1,0:T(8,128)(2,1)S(1)} %get-tuple-element.11), channel_id=1, replica_groups=mesh['fs'=32,'tp'=8] {'fs'}, dimensions={0} | all-to-all | bytes 1048576 | tf_op jit(solution)/shard_map/all_to_all | solution.py:34
  136.8 5.0 %all-to-all-start.1 = ((bf16[32,1,2,32,128]{4,3,2,1,0:T(8,128)(2,1)}), bf16[32,1,2,32,128]{4,3,2,1,0:T(8,128)(2,1)S(1)}, u32[]{:S(2)}, u32[]{:S(2)}) async-start(bf16[32,1,2,32,128]{4,3,2,1,0:T(8,128)(2,1)} %get-tuple-element.12), calls=%async_computation.1 | async-start | bytes 1048576 | tf_op jit(solution)/shard_map/all_to_all | solution.py:34
  141.8 0.9 fusion.35
  142.8 15.6 %all-to-all-done.1 = bf16[32,1,2,32,128]{4,3,2,1,0:T(8,128)(2,1)S(1)} async-done(((bf16[32,1,2,32,128]{4,3,2,1,0:T(8,128)(2,1)}), bf16[32,1,2,32,128]{4,3,2,1,0:T(8,128)(2,1)S(1)}, u32[]{:S(2)}, u32[]{:S(2)}) %all-to-all-start.1) | async-done | bytes 524320 | tf_op jit(solution)/shard_map/all_to_all | solution.py:34
  158.4 21.5 %all_to_all.46 = bf16[32,1,2,32,128]{4,3,2,1,0:T(8,128)(2,1)S(1)} all-to-all(bf16[32,1,2,32,128]{4,3,2,1,0:T(8,128)(2,1)S(1)} %get-tuple-element.9), channel_id=1, replica_groups=mesh['fs'=32,'tp'=8] {'fs'}, dimensions={0} | all-to-all | bytes 1048576 | tf_op jit(solution)/shard_map/all_to_all | solution.py:34
  179.9 5.1 %all-to-all-start.3 = ((bf16[32,1,2,32,128]{4,3,2,1,0:T(8,128)(2,1)}), bf16[32,1,2,32,128]{4,3,2,1,0:T(8,128)(2,1)S(1)}, u32[]{:S(2)}, u32[]{:S(2)}) async-start(bf16[32,1,2,32,128]{4,3,2,1,0:T(8,128)(2,1)} %get-tuple-element.10), calls=%async_computation.3 | async-start | bytes 1048576 | tf_op jit(solution)/shard_map/all_to_all | solution.py:34
  185.5 16.0 %all-to-all-done.3 = bf16[32,1,2,32,128]{4,3,2,1,0:T(8,128)(2,1)S(1)} async-done(((bf16[32,1,2,32,128]{4,3,2,1,0:T(8,128)(2,1)}), bf16[32,1,2,32,128]{4,3,2,1,0:T(8,128)(2,1)S(1)}, u32[]{:S(2)}, u32[]{:S(2)}) %all-to-all-start.3) | async-done | bytes 524320 | tf_op jit(solution)/shard_map/all_to_all | solution.py:34
  201.7 1.6 fusion.34
  204.5 18.0 %all-gather.6.cloned.1.call-done = bf16[32,2,48,2048]{3,0,1,2:T(8,128)(2,1)} async-done(((bf16[32,2,6,2048]{3,0,1,2:T(8,128)(2,1)}), bf16[32,2,48,2048]{3,0,1,2:T(8,128)(2,1)}) %all-gather.6.cloned.1.call-update) | async-done | bytes 12582928 | tf_op jit(solution)/shard_map/all_gather | solution.py:116
  222.5 18.0 %fusion.2 = f32[2,128,32,48]{1,3,2,0:T(8,128)S(1)} fusion(bf16[2,2048,128,1]{2,1,3,0:T(8,128)(2,1)S(1)} %bitcast.105, bf16[32,2,48,2048]{3,0,1,2:T(8,128)(2,1)} %all-gather.6.cloned.1.call-done), kind=kOutput, calls=%fused_computation.5 | convolution fusion | flops 1610612736 | bytes 15204352 | tf_op jit(solution)/shard_map/secn,enf->secf/dot_general | solution.py:62
  240.6 13.8 %fusion.13 = bf16[128,32,2,48]{0,3,1,2:T(8,128)(2,1)S(1)} fusion(f32[2,128,32,48]{1,3,2,0:T(8,128)S(1)} %fusion.2, bf16[2,2048,128,1]{2,1,3,0:T(8,128)(2,1)S(1)} %bitcast.107, bf16[32,2,48,2048]{3,0,1,2:T(8,128)(2,1)} %all-gather.6.cloned.1.call-done), kind=kOutput, calls=%fused_computation.20 | convolution fusion | flops 1612972032 | bytes 15990784 | tf_op jit(solution)/shard_map/secn,enf->secf/dot_general | solution.py:63
  254.4 0.9 pad_maximum_fusion
  255.4 0.9 copy-done.1
  256.4 37.4 %all_to_all.47 = bf16[32,2,32,256]{3,2,1,0:T(8,128)(2,1)S(1)} all-to-all(bf16[32,2,32,256]{3,2,1,0:T(8,128)(2,1)S(1)} %bitcast.101), channel_id=1, replica_groups=mesh['fs'=32,'tp'=8] {'fs'}, dimensions={0} | all-to-all | bytes 2097152 | tf_op jit(solution)/shard_map/all_to_all | solution.py:120
  293.9 10.6 %all-gather.8.cloned.1.call-done = bf16[1024,3264]{0,1:T(8,128)(2,1)} async-done(((bf16[128,3264]{0,1:T(8,128)(2,1)}), bf16[1024,3264]{0,1:T(8,128)(2,1)}) %all-gather.8.cloned.1.call-update) | async-done | bytes 6684688 | tf_op jit(solution)/shard_map/all_gather | solution.py:51
  304.6 2.8 slice-done
  307.4 1.8 fusion.17
  309.2 1.4 copy.70
  310.6 10.2 %all-to-all-start.6 = ((bf16[32,2,48,256]{3,2,1,0:T(8,128)(2,1)}), bf16[32,2,48,256]{3,2,1,0:T(8,128)(2,1)S(1)}, u32[]{:S(2)}, u32[]{:S(2)}) async-start(bf16[32,2,48,256]{3,2,1,0:T(8,128)(2,1)} %copy.70), calls=%async_computation.6 | async-start | bytes 3145728 | tf_op jit(solution)/shard_map/all_to_all | solution.py:130
  320.9 79.3 %all_gather.13 = bf16[1024,256]{1,0:T(8,128)(2,1)S(1)} all-gather(bf16[32,256]{1,0:T(8,128)(2,1)S(1)} %convert_element_type.57), channel_id=1, replica_groups=mesh['fs'=32,'tp'=8] {'fs'}, dimensions={0}, use_global_device_ids=true | all-gather | bytes 540672 | tf_op jit(solution)/shard_map/all_gather | solution.py:101
  400.3 4.8 %gather_fusion.1 = bf16[1536,256]{1,0:T(8,128)(2,1)S(1)} fusion(bf16[3072,256]{1,0:T(8,128)(2,1)S(1)} %bitcast.96, s32[2048]{0:T(1024)S(1)} %pad_clamp_fusion), kind=kCustom, calls=%fused_computation.1 | custom fusion | bytes 1579008 | tf_op jit(solution)/shard_map/gather | solution.py:135
  405.6 1.9 fusion.22
  (76 shorter events, 7.4 us)
Async XLA Ops:
  8.3 19.2 %copy-start.13 = (s32[2]{0:T(128)S(1)}, s32[2]{0:T(128)}, u32[]{:S(2)}) copy-start(s32[2]{0:T(128)} %constant.57) | copy-start | bytes 28
  8.4 19.3 %copy-start.12 = (s32[2]{0:T(128)S(1)}, s32[2]{0:T(128)}, u32[]{:S(2)}) copy-start(s32[2]{0:T(128)} %constant.60) | copy-start | bytes 28
  8.4 25.9 %copy-start = (bf16[192,2048]{1,0:T(8,128)(2,1)S(1)}, bf16[192,2048]{1,0:T(8,128)(2,1)}, u32[]{:S(2)}) copy-start(bf16[192,2048]{1,0:T(8,128)(2,1)} %param.10) | copy-start | bytes 2359300
  56.5 11.4 %copy-start.7 = (f32[64,128]{1,0:T(8,128)S(1)}, f32[64,128]{1,0:T(8,128)}, u32[]{:S(2)}) copy-start(f32[64,128]{1,0:T(8,128)} %param.15) | copy-start | bytes 98308
  56.5 11.4 %copy-start.8 = (f32[64,128]{1,0:T(8,128)S(1)}, f32[64,128]{1,0:T(8,128)}, u32[]{:S(2)}) copy-start(f32[64,128]{1,0:T(8,128)} %param.16) | copy-start | bytes 98308
  56.5 11.4 %copy-start.11 = (f32[64]{0:T(128)S(1)}, f32[64]{0:T(128)}, u32[]{:S(2)}) copy-start(f32[64]{0:T(128)} %param.11) | copy-start | bytes 772
  56.5 50.6 %all-to-all-start.5 = ((bf16[32,2,6,2048]{3,1,2,0:T(2,128)(2,1)}), bf16[32,2,6,2048]{3,1,2,0:T(2,128)(2,1)S(1)}, u32[]{:S(2)}, u32[]{:S(2)}) async-start(bf16[32,2,6,2048]{3,1,2,0:T(2,128)(2,1)} %copy.64), calls=%async_computation.5 | async-start | bytes 3145728 | tf_op jit(solution)/shard_map/all_to_all | solution.py:115
  67.8 133.9 %all-gather.4.cloned.1.call-start = ((), (), s32[]{:S(2)}) async-start(), calls=%async_computation.7 | async-start | bytes 1081344 | tf_op jit(solution)/shard_map/all_gather | solution.py:44
  68.6 153.9 %all-gather.6.cloned.1.call-start = ((), (), s32[]{:S(2)}) async-start(), calls=%async_computation.8 | async-start | bytes 14155776 | tf_op jit(solution)/shard_map/all_gather | solution.py:116
  136.8 21.6 %all-to-all-start.1 = ((bf16[32,1,2,32,128]{4,3,2,1,0:T(8,128)(2,1)}), bf16[32,1,2,32,128]{4,3,2,1,0:T(8,128)(2,1)S(1)}, u32[]{:S(2)}, u32[]{:S(2)}) async-start(bf16[32,1,2,32,128]{4,3,2,1,0:T(8,128)(2,1)} %get-tuple-element.12), calls=%async_computation.1 | async-start | bytes 1048576 | tf_op jit(solution)/shard_map/all_to_all | solution.py:34
  179.9 21.5 %all-to-all-start.3 = ((bf16[32,1,2,32,128]{4,3,2,1,0:T(8,128)(2,1)}), bf16[32,1,2,32,128]{4,3,2,1,0:T(8,128)(2,1)S(1)}, u32[]{:S(2)}, u32[]{:S(2)}) async-start(bf16[32,1,2,32,128]{4,3,2,1,0:T(8,128)(2,1)} %get-tuple-element.10), calls=%async_computation.3 | async-start | bytes 1048576 | tf_op jit(solution)/shard_map/all_to_all | solution.py:34
  185.0 119.6 %all-gather.8.cloned.1.call-start = ((), (), s32[]{:S(2)}) async-start(), calls=%async_computation.9 | async-start | bytes 7520256 | tf_op jit(solution)/shard_map/all_gather | solution.py:51
  185.4 37.0 %copy-start.3 = (bf16[1,2,32,64,128]{4,3,2,1,0:T(8,128)(2,1)}, bf16[1,2,32,64,128]{4,3,2,1,0:T(8,128)(2,1)S(1)}, u32[]{:S(2)}) copy-start(bf16[1,2,32,64,128]{4,3,2,1,0:T(8,128)(2,1)S(1)} %copy.55) | copy-start | bytes 3145732
  201.6 38.9 %copy-start.4 = (bf16[1,2,32,64,128]{4,3,2,1,0:T(8,128)(2,1)}, bf16[1,2,32,64,128]{4,3,2,1,0:T(8,128)(2,1)S(1)}, u32[]{:S(2)}) copy-start(bf16[1,2,32,64,128]{4,3,2,1,0:T(8,128)(2,1)S(1)} %copy.56) | copy-start | bytes 3145732
  203.3 0.8 copy-start.6
  203.3 37.2 %copy-start.2 = (bf16[2048,128]{1,0:T(8,128)(2,1)}, bf16[2048,128]{1,0:T(8,128)(2,1)S(1)}, u32[]{:S(2)}) copy-start(bf16[2048,128]{1,0:T(8,128)(2,1)S(1)} %get-tuple-element.34) | copy-start | bytes 1572868
  254.3 1.9 copy-start.1
  293.9 10.7 %copy-start.5 = (bf16[1,2,32,32,256]{4,3,2,1,0:T(8,128)(2,1)}, bf16[1,2,32,32,256]{4,3,2,1,0:T(8,128)(2,1)S(1)}, u32[]{:S(2)}) copy-start(bf16[1,2,32,32,256]{4,3,2,1,0:T(8,128)(2,1)S(1)} %copy.57) | copy-start | bytes 3145732
  304.6 2.8 slice-start
  310.6 10.2 %copy-start.10 = (f32[192,8]{0,1:T(8,128)S(1)}, f32[192,8]{0,1:T(8,128)}, u32[]{:S(2)}) copy-start(f32[192,8]{0,1:T(8,128)} %param.19) | copy-start | bytes 18436
  310.6 10.3 %copy-start.9 = (f32[32,256]{1,0:T(8,128)S(1)}, f32[32,256]{1,0:T(8,128)}, u32[]{:S(2)}) copy-start(f32[32,256]{1,0:T(8,128)} %param.17) | copy-start | bytes 98308
  310.6 89.7 %all-to-all-start.6 = ((bf16[32,2,48,256]{3,2,1,0:T(8,128)(2,1)}), bf16[32,2,48,256]{3,2,1,0:T(8,128)(2,1)S(1)}, u32[]{:S(2)}, u32[]{:S(2)}) async-start(bf16[32,2,48,256]{3,2,1,0:T(8,128)(2,1)} %copy.70), calls=%async_computation.6 | async-start | bytes 3145728 | tf_op jit(solution)/shard_map/all_to_all | solution.py:130
Sparse Core Ops, SparseCore 0:
  71.8 80.5 all-gather.3
  154.2 68.2 all-gather.5
  255.5 49.0 all-gather.7
where the time goes:
time: 416 us; the launch traced here: 415 us
  blocking collectives  162 us (39%)
  waiting for transfers between devices  98.7 us (24%)
  local copies, waits for them, and re-layouts  46.8 us (11%)
  matrix products  36.3 us (9%)
  starting transfers between devices  31.9 us (8%)
  other arithmetic  24.6 us (6%)
  between operations  14.2 us (3%)
    all_gather x1, blocking collectives, body(): lax.all_gather(shared_third_local, 'fs', axis=0, tiled=True)  79.3 us
    all_to_all x2, blocking collectives, several_exchanges(): lax.all_to_all(share, axis, split_axis=0, concat_axis=0, tiled=True)  45.4 us
    all_to_all x1, waiting for transfers between devices, body(): lax.all_to_all(mine, 'fs', split_axis=0, concat_axis=0, tiled=True)  38.4 us
    all_to_all x1, blocking collectives, body(): lax.all_to_all(down_local, 'fs', split_axis=0, concat_axis=2, tiled=True)  37.4 us
    all_to_all x2, waiting for transfers between devices, several_exchanges(): lax.all_to_all(share, axis, split_axis=0, concat_axis=0, tiled=True)  31.6 us
    another operation x3, other arithmetic  18.4 us
    dot_general x1, matrix products, expert_hidden(): jnp.einsum('secn,enf->secf', rows, gate_new, preferred_element_type=jnp.f...  18 us
    all_gather x1, waiting for transfers between devices, body(): lax.all_gather(arrived, 'tp', axis=2, tiled=True)  18 us
  transfers between devices with their start and end apart: 7, of which 5 were waited for; matrix products, arithmetic and copies ran while one was open for 3% of the time, Pallas kernels for 0%

commit v1 on v0

--- a/solution.py
+++ b/solution.py
@@ -98,7 +98,10 @@
     up_ready = up_moved[0]
     shared_gate_ready, shared_up_ready, shared_down_ready = (
         *side_by_side((shared_first_local, shared_second_local), "fs", 0, 1),
-        lax.all_gather(shared_third_local, "fs", axis=0, tiled=True),
+        jnp.concatenate(
+            lax.all_to_all(jnp.stack([shared_third_local] * lax.axis_size("fs")), "fs", 0, 0),
+            axis=0,
+        ),
     )
     wide = tokens.astype(jnp.float32)
     normed = (wide * lax.rsqrt(jnp.mean(wide * wide, axis=-1, keepdims=True) + EPS)).astype(

time: 416 us -> 378 us (0.909)
  blocking collectives: 162 us -> 45.4 us
  waiting for transfers between devices: 98.7 us -> 163 us
  starting transfers between devices: 31.9 us -> 43.4 us
    all_gather x1 -> x0, blocking collectives: 79.3 us -> none  [body(): lax.all_gather(shared_third_local, 'fs', axis=0, tiled=True)]
    all_to_all x1 -> x0, blocking collectives: 37.4 us -> none  [body(): lax.all_to_all(down_local, 'fs', split_axis=0, concat_axis=2, tiled=True)]
    all_to_all x1, waiting for transfers between devices: 0.01 us -> 37.3 us  [body(): lax.all_to_all(routed_total.astype(jnp.bfloat16), 'fs', split_axis=0, con...]
    all_to_all x0 -> x2, waiting for transfers between devices: none -> 35.6 us  [the longest x1 27.6 us: body(): lax.all_to_all(down_local, 'fs', split_axis=0, concat_axis=2, tiled=True)]
    all_to_all x0 -> x2, starting transfers between devices: none -> 16.5 us  [the longest x1 10.1 us: body(): lax.all_to_all(down_local, 'fs', split_axis=0, concat_axis=2, tiled=True)]
    all_gather x1, waiting for transfers between devices: 10.6 us -> 2.14 us  [turned_gather(): result = lax.all_gather(both, axis, axis=0, tiled=True)]
    all_to_all x1, starting transfers between devices: 10.2 us -> 5.12 us  [body(): lax.all_to_all(routed_total.astype(jnp.bfloat16), 'fs', split_axis=0, con...]
  transfers between devices with their start and end apart: 7 -> 9, of which waited for: 5 -> 8; matrix products, arithmetic and copies ran while one was open for 3% -> 4% of each run, Pallas kernels for 0% -> 0%
where the time goes in v1:
time: 378 us; the launch traced here: 376 us
  waiting for transfers between devices  163 us (43%)
  local copies, waits for them, and re-layouts  47.7 us (13%)
  blocking collectives  45.4 us (12%)
  starting transfers between devices  43.4 us (11%)
  matrix products  36.3 us (10%)
  other arithmetic  25.6 us (7%)
  between operations  14.2 us (4%)
    all_to_all x2, blocking collectives, several_exchanges(): lax.all_to_all(share, axis, split_axis=0, concat_axis=0, tiled=True)  45.4 us
    all_to_all x1, waiting for transfers between devices, body(): lax.all_to_all(mine, 'fs', split_axis=0, concat_axis=0, tiled=True)  38.4 us
    all_to_all x1, waiting for transfers between devices, body(): lax.all_to_all(routed_total.astype(jnp.bfloat16), 'fs', split_axis=0, con...  37.3 us
    all_to_all x2, waiting for transfers between devices, several_exchanges(): lax.all_to_all(share, axis, split_axis=0, concat_axis=0, tiled=True)  31.6 us
    all_to_all x1, waiting for transfers between devices, body(): lax.all_to_all(down_local, 'fs', split_axis=0, concat_axis=2, tiled=True)  27.6 us
    another operation x3, other arithmetic  18.4 us
    dot_general x1, matrix products, expert_hidden(): jnp.einsum('secn,enf->secf', rows, gate_new, preferred_element_type=jnp.f...  18 us
    all_gather x1, waiting for transfers between devices, body(): lax.all_gather(arrived, 'tp', axis=2, tiled=True)  18 us
  transfers between devices with their start and end apart: 9, of which 8 were waited for; matrix products, arithmetic and copies ran while one was open for 4% of the time, Pallas kernels for 0%

profile of v1, /device:TPU:32, one launch (start us, length us, event | category | flops | bytes accessed | tf_op | source)
XLA Modules:
  0.0 375.7 jit_solution(5297712242450986957)
XLA Ops:
  8.4 18.1 %reduce-window.6 = s32[64,12,128]{2,1,0:T(8,128)S(1)} reduce-window(s32[64,12,128]{2,1,0:T(8,128)S(1)} %fusion.25, s32[]{:T(128)} %constant.44.clone.1), window={size=1x1x128 pad=0_0x0_0x127_0}, to_apply=%region_1.0 | reduce-window | flops 12484608 | bytes 786436 | tf_op jit(solution)/shard_map/reduce-window
  27.8 6.2 %scatter_custom_fusion = s32[3072]{0:T(1024)S(1)} fusion(s32[1536]{0:T(1024)S(1)} %get-tuple-element.23, s32[1536]{0:T(1024)S(1)} %get-tuple-element.22, s32[]{:T(128)} %constant.44.clone.1), kind=kCustom, calls=%fused_computation.63 | custom fusion | bytes 12292
  34.7 15.9 %gather_fusion = bf16[3072,2048]{1,0:T(8,128)(2,1)} fusion(bf16[192,2048]{1,0:T(8,128)(2,1)S(1)} %fusion.11, s32[3072]{0:T(1024)S(1)} %broadcast_clamp_fusion), kind=kCustom, calls=%fused_computation | custom fusion | bytes 25178112 | tf_op jit(solution)/shard_map/gather | solution.py:115
  50.6 3.0 constant_dynamic-slice_fusion
  53.6 2.8 copy.64
  56.4 11.3 %all-to-all-start.6 = ((bf16[32,2,6,2048]{3,1,2,0:T(2,128)(2,1)}), bf16[32,2,6,2048]{3,1,2,0:T(2,128)(2,1)S(1)}, u32[]{:S(2)}, u32[]{:S(2)}) async-start(bf16[32,2,6,2048]{3,1,2,0:T(2,128)(2,1)} %copy.64), calls=%async_computation.6 | async-start | bytes 3145728 | tf_op jit(solution)/shard_map/all_to_all | solution.py:118
  68.6 38.4 %all-to-all-done.6 = bf16[32,2,6,2048]{3,1,2,0:T(2,128)(2,1)S(1)} async-done(((bf16[32,2,6,2048]{3,1,2,0:T(2,128)(2,1)}), bf16[32,2,6,2048]{3,1,2,0:T(2,128)(2,1)S(1)}, u32[]{:S(2)}, u32[]{:S(2)}) %all-to-all-start.6) | async-done | bytes 1572896 | tf_op jit(solution)/shard_map/all_to_all | solution.py:118
  107.1 2.1 copy.65
  109.1 2.8 multiply_convert_fusion
  112.9 23.9 %all_to_all.50 = bf16[32,1,2,32,128]{4,3,2,1,0:T(8,128)(2,1)S(1)} all-to-all(bf16[32,1,2,32,128]{4,3,2,1,0:T(8,128)(2,1)S(1)} %get-tuple-element.11), channel_id=1, replica_groups=mesh['fs'=32,'tp'=8] {'fs'}, dimensions={0} | all-to-all | bytes 1048576 | tf_op jit(solution)/shard_map/all_to_all | solution.py:34
  136.8 5.0 %all-to-all-start.1 = ((bf16[32,1,2,32,128]{4,3,2,1,0:T(8,128)(2,1)}), bf16[32,1,2,32,128]{4,3,2,1,0:T(8,128)(2,1)S(1)}, u32[]{:S(2)}, u32[]{:S(2)}) async-start(bf16[32,1,2,32,128]{4,3,2,1,0:T(8,128)(2,1)} %get-tuple-element.12), calls=%async_computation.1 | async-start | bytes 1048576 | tf_op jit(solution)/shard_map/all_to_all | solution.py:34
  142.8 15.6 %all-to-all-done.1 = bf16[32,1,2,32,128]{4,3,2,1,0:T(8,128)(2,1)S(1)} async-done(((bf16[32,1,2,32,128]{4,3,2,1,0:T(8,128)(2,1)}), bf16[32,1,2,32,128]{4,3,2,1,0:T(8,128)(2,1)S(1)}, u32[]{:S(2)}, u32[]{:S(2)}) %all-to-all-start.1) | async-done | bytes 524320 | tf_op jit(solution)/shard_map/all_to_all | solution.py:34
  158.4 21.5 %all_to_all.51 = bf16[32,1,2,32,128]{4,3,2,1,0:T(8,128)(2,1)S(1)} all-to-all(bf16[32,1,2,32,128]{4,3,2,1,0:T(8,128)(2,1)S(1)} %get-tuple-element.9), channel_id=1, replica_groups=mesh['fs'=32,'tp'=8] {'fs'}, dimensions={0} | all-to-all | bytes 1048576 | tf_op jit(solution)/shard_map/all_to_all | solution.py:34
  179.9 5.1 %all-to-all-start.3 = ((bf16[32,1,2,32,128]{4,3,2,1,0:T(8,128)(2,1)}), bf16[32,1,2,32,128]{4,3,2,1,0:T(8,128)(2,1)S(1)}, u32[]{:S(2)}, u32[]{:S(2)}) async-start(bf16[32,1,2,32,128]{4,3,2,1,0:T(8,128)(2,1)} %get-tuple-element.10), calls=%async_computation.3 | async-start | bytes 1048576 | tf_op jit(solution)/shard_map/all_to_all | solution.py:34
  185.5 16.0 %all-to-all-done.3 = bf16[32,1,2,32,128]{4,3,2,1,0:T(8,128)(2,1)S(1)} async-done(((bf16[32,1,2,32,128]{4,3,2,1,0:T(8,128)(2,1)}), bf16[32,1,2,32,128]{4,3,2,1,0:T(8,128)(2,1)S(1)}, u32[]{:S(2)}, u32[]{:S(2)}) %all-to-all-start.3) | async-done | bytes 524320 | tf_op jit(solution)/shard_map/all_to_all | solution.py:34
  201.7 1.6 fusion.34
  204.5 18.0 %all-gather.6.cloned.1.call-done = bf16[32,2,48,2048]{3,0,1,2:T(8,128)(2,1)} async-done(((bf16[32,2,6,2048]{3,0,1,2:T(8,128)(2,1)}), bf16[32,2,48,2048]{3,0,1,2:T(8,128)(2,1)}) %all-gather.6.cloned.1.call-update) | async-done | bytes 12582928 | tf_op jit(solution)/shard_map/all_gather | solution.py:119
  222.5 18.0 %fusion.2 = f32[2,128,32,48]{1,3,2,0:T(8,128)S(1)} fusion(bf16[2,2048,128,1]{2,1,3,0:T(8,128)(2,1)S(1)} %bitcast.107, bf16[32,2,48,2048]{3,0,1,2:T(8,128)(2,1)} %all-gather.6.cloned.1.call-done), kind=kOutput, calls=%fused_computation.5 | convolution fusion | flops 1610612736 | bytes 15204352 | tf_op jit(solution)/shard_map/secn,enf->secf/dot_general | solution.py:62
  240.6 13.8 %fusion.13 = bf16[128,32,2,48]{0,3,1,2:T(8,128)(2,1)S(1)} fusion(f32[2,128,32,48]{1,3,2,0:T(8,128)S(1)} %fusion.2, bf16[2,2048,128,1]{2,1,3,0:T(8,128)(2,1)S(1)} %bitcast.109, bf16[32,2,48,2048]{3,0,1,2:T(8,128)(2,1)} %all-gather.6.cloned.1.call-done), kind=kOutput, calls=%fused_computation.20 | convolution fusion | flops 1612972032 | bytes 15990784 | tf_op jit(solution)/shard_map/secn,enf->secf/dot_general | solution.py:63
  256.2 1.1 convert_element_type.54
  257.4 10.1 %all-to-all-start.4 = ((bf16[32,2,32,256]{3,2,1,0:T(8,128)(2,1)}), bf16[32,2,32,256]{3,2,1,0:T(8,128)(2,1)S(1)}, u32[]{:S(2)}, u32[]{:S(2)}) async-start(bf16[32,2,32,256]{3,2,1,0:T(8,128)(2,1)} %bitcast.6), calls=%async_computation.4 | async-start | bytes 2097152 | tf_op jit(solution)/shard_map/all_to_all | solution.py:123
  267.4 27.6 %all-to-all-done.4 = bf16[32,2,32,256]{3,2,1,0:T(8,128)(2,1)S(1)} async-done(((bf16[32,2,32,256]{3,2,1,0:T(8,128)(2,1)}), bf16[32,2,32,256]{3,2,1,0:T(8,128)(2,1)S(1)}, u32[]{:S(2)}, u32[]{:S(2)}) %all-to-all-start.4) | async-done | bytes 1048608 | tf_op jit(solution)/shard_map/all_to_all | solution.py:123
  295.9 6.5 %all-to-all-start.5 = ((bf16[32,32,256]{2,1,0:T(8,128)(2,1)}), bf16[32,32,256]{2,1,0:T(8,128)(2,1)S(1)}, u32[]{:S(2)}, u32[]{:S(2)}) async-start(bf16[32,32,256]{2,1,0:T(8,128)(2,1)} %stack.2), calls=%async_computation.5 | async-start | bytes 1048576 | tf_op jit(solution)/shard_map/all_to_all | solution.py:102
  302.4 2.1 all-gather.8.cloned.1.call-done
  304.6 2.8 slice-done
  307.4 1.8 fusion.17
  309.2 1.4 copy.70
  310.6 8.0 %all-to-all-done.5 = bf16[32,32,256]{2,1,0:T(8,128)(2,1)S(1)} async-done(((bf16[32,32,256]{2,1,0:T(8,128)(2,1)}), bf16[32,32,256]{2,1,0:T(8,128)(2,1)S(1)}, u32[]{:S(2)}, u32[]{:S(2)}) %all-to-all-start.5) | async-done | bytes 524320 | tf_op jit(solution)/shard_map/all_to_all | solution.py:102
  318.6 5.1 %all-to-all-start.7 = ((bf16[32,2,48,256]{3,2,1,0:T(8,128)(2,1)}), bf16[32,2,48,256]{3,2,1,0:T(8,128)(2,1)S(1)}, u32[]{:S(2)}, u32[]{:S(2)}) async-start(bf16[32,2,48,256]{3,2,1,0:T(8,128)(2,1)} %copy.70), calls=%async_computation.7 | async-start | bytes 3145728 | tf_op jit(solution)/shard_map/all_to_all | solution.py:133
  323.9 37.3 %all-to-all-done.7 = bf16[32,2,48,256]{3,2,1,0:T(8,128)(2,1)S(1)} async-done(((bf16[32,2,48,256]{3,2,1,0:T(8,128)(2,1)}), bf16[32,2,48,256]{3,2,1,0:T(8,128)(2,1)S(1)}, u32[]{:S(2)}, u32[]{:S(2)}) %all-to-all-start.7) | async-done | bytes 1572896 | tf_op jit(solution)/shard_map/all_to_all | solution.py:133
  361.2 4.8 %gather_fusion.1 = bf16[1536,256]{1,0:T(8,128)(2,1)S(1)} fusion(bf16[3072,256]{1,0:T(8,128)(2,1)S(1)} %bitcast.97, s32[2048]{0:T(1024)S(1)} %pad_clamp_fusion), kind=kCustom, calls=%fused_computation.1 | custom fusion | bytes 1579008 | tf_op jit(solution)/shard_map/gather | solution.py:138
  366.5 1.9 fusion.22
  (79 shorter events, 11.8 us)
Async XLA Ops:
  8.3 19.2 %copy-start.13 = (s32[2]{0:T(128)S(1)}, s32[2]{0:T(128)}, u32[]{:S(2)}) copy-start(s32[2]{0:T(128)} %constant.57) | copy-start | bytes 28
  8.4 19.3 %copy-start.12 = (s32[2]{0:T(128)S(1)}, s32[2]{0:T(128)}, u32[]{:S(2)}) copy-start(s32[2]{0:T(128)} %constant.60) | copy-start | bytes 28
  8.4 25.9 %copy-start = (bf16[192,2048]{1,0:T(8,128)(2,1)S(1)}, bf16[192,2048]{1,0:T(8,128)(2,1)}, u32[]{:S(2)}) copy-start(bf16[192,2048]{1,0:T(8,128)(2,1)} %param.10) | copy-start | bytes 2359300
  56.4 11.4 %copy-start.7 = (f32[64,128]{1,0:T(8,128)S(1)}, f32[64,128]{1,0:T(8,128)}, u32[]{:S(2)}) copy-start(f32[64,128]{1,0:T(8,128)} %param.15) | copy-start | bytes 98308
  56.4 11.4 %copy-start.8 = (f32[64,128]{1,0:T(8,128)S(1)}, f32[64,128]{1,0:T(8,128)}, u32[]{:S(2)}) copy-start(f32[64,128]{1,0:T(8,128)} %param.16) | copy-start | bytes 98308
  56.4 11.4 %copy-start.11 = (f32[64]{0:T(128)S(1)}, f32[64]{0:T(128)}, u32[]{:S(2)}) copy-start(f32[64]{0:T(128)} %param.11) | copy-start | bytes 772
  56.4 50.6 %all-to-all-start.6 = ((bf16[32,2,6,2048]{3,1,2,0:T(2,128)(2,1)}), bf16[32,2,6,2048]{3,1,2,0:T(2,128)(2,1)S(1)}, u32[]{:S(2)}, u32[]{:S(2)}) async-start(bf16[32,2,6,2048]{3,1,2,0:T(2,128)(2,1)} %copy.64), calls=%async_computation.6 | async-start | bytes 3145728 | tf_op jit(solution)/shard_map/all_to_all | solution.py:118
  67.8 133.9 %all-gather.4.cloned.1.call-start = ((), (), s32[]{:S(2)}) async-start(), calls=%async_computation.8 | async-start | bytes 1081344 | tf_op jit(solution)/shard_map/all_gather | solution.py:44
  68.6 153.9 %all-gather.6.cloned.1.call-start = ((), (), s32[]{:S(2)}) async-start(), calls=%async_computation.9 | async-start | bytes 14155776 | tf_op jit(solution)/shard_map/all_gather | solution.py:119
  136.8 21.6 %all-to-all-start.1 = ((bf16[32,1,2,32,128]{4,3,2,1,0:T(8,128)(2,1)}), bf16[32,1,2,32,128]{4,3,2,1,0:T(8,128)(2,1)S(1)}, u32[]{:S(2)}, u32[]{:S(2)}) async-start(bf16[32,1,2,32,128]{4,3,2,1,0:T(8,128)(2,1)} %get-tuple-element.12), calls=%async_computation.1 | async-start | bytes 1048576 | tf_op jit(solution)/shard_map/all_to_all | solution.py:34
  179.9 21.5 %all-to-all-start.3 = ((bf16[32,1,2,32,128]{4,3,2,1,0:T(8,128)(2,1)}), bf16[32,1,2,32,128]{4,3,2,1,0:T(8,128)(2,1)S(1)}, u32[]{:S(2)}, u32[]{:S(2)}) async-start(bf16[32,1,2,32,128]{4,3,2,1,0:T(8,128)(2,1)} %get-tuple-element.10), calls=%async_computation.3 | async-start | bytes 1048576 | tf_op jit(solution)/shard_map/all_to_all | solution.py:34
  185.0 119.6 %all-gather.8.cloned.1.call-start = ((), (), s32[]{:S(2)}) async-start(), calls=%async_computation.10 | async-start | bytes 7520256 | tf_op jit(solution)/shard_map/all_gather | solution.py:51
  185.4 37.0 %copy-start.3 = (bf16[1,2,32,64,128]{4,3,2,1,0:T(8,128)(2,1)}, bf16[1,2,32,64,128]{4,3,2,1,0:T(8,128)(2,1)S(1)}, u32[]{:S(2)}) copy-start(bf16[1,2,32,64,128]{4,3,2,1,0:T(8,128)(2,1)S(1)} %copy.55) | copy-start | bytes 3145732
  201.6 38.9 %copy-start.4 = (bf16[1,2,32,64,128]{4,3,2,1,0:T(8,128)(2,1)}, bf16[1,2,32,64,128]{4,3,2,1,0:T(8,128)(2,1)S(1)}, u32[]{:S(2)}) copy-start(bf16[1,2,32,64,128]{4,3,2,1,0:T(8,128)(2,1)S(1)} %copy.56) | copy-start | bytes 3145732
  203.3 0.8 copy-start.6
  203.3 37.2 %copy-start.2 = (bf16[2048,128]{1,0:T(8,128)(2,1)}, bf16[2048,128]{1,0:T(8,128)(2,1)S(1)}, u32[]{:S(2)}) copy-start(bf16[2048,128]{1,0:T(8,128)(2,1)S(1)} %get-tuple-element.34) | copy-start | bytes 1572868
  254.3 1.9 copy-start.1
  256.2 11.2 %copy-start.9 = (f32[32,256]{1,0:T(8,128)S(1)}, f32[32,256]{1,0:T(8,128)}, u32[]{:S(2)}) copy-start(f32[32,256]{1,0:T(8,128)} %param.17) | copy-start | bytes 98308
  257.4 37.7 %all-to-all-start.4 = ((bf16[32,2,32,256]{3,2,1,0:T(8,128)(2,1)}), bf16[32,2,32,256]{3,2,1,0:T(8,128)(2,1)S(1)}, u32[]{:S(2)}, u32[]{:S(2)}) async-start(bf16[32,2,32,256]{3,2,1,0:T(8,128)(2,1)} %bitcast.6), calls=%async_computation.4 | async-start | bytes 2097152 | tf_op jit(solution)/shard_map/all_to_all | solution.py:123
  295.9 22.8 %all-to-all-start.5 = ((bf16[32,32,256]{2,1,0:T(8,128)(2,1)}), bf16[32,32,256]{2,1,0:T(8,128)(2,1)S(1)}, u32[]{:S(2)}, u32[]{:S(2)}) async-start(bf16[32,32,256]{2,1,0:T(8,128)(2,1)} %stack.2), calls=%async_computation.5 | async-start | bytes 1048576 | tf_op jit(solution)/shard_map/all_to_all | solution.py:102
  302.4 2.2 copy-start.5
  304.6 2.8 slice-start
  310.6 13.2 %copy-start.10 = (f32[192,8]{0,1:T(8,128)S(1)}, f32[192,8]{0,1:T(8,128)}, u32[]{:S(2)}) copy-start(f32[192,8]{0,1:T(8,128)} %param.19) | copy-start | bytes 18436
  318.6 42.6 %all-to-all-start.7 = ((bf16[32,2,48,256]{3,2,1,0:T(8,128)(2,1)}), bf16[32,2,48,256]{3,2,1,0:T(8,128)(2,1)S(1)}, u32[]{:S(2)}, u32[]{:S(2)}) async-start(bf16[32,2,48,256]{3,2,1,0:T(8,128)(2,1)} %copy.70), calls=%async_computation.7 | async-start | bytes 3145728 | tf_op jit(solution)/shard_map/all_to_all | solution.py:133
Sparse Core Ops, SparseCore 0:
  71.7 80.5 all-gather.3
  154.2 68.2 all-gather.5
  255.5 49.0 all-gather.7
